TPU v7x, 32 devices: a whole 2x2x4 slice. The times are simulated.
32 devices in a mesh: sp: 16 (over z, y, core), dp: 2 (over x).
Axes of the slice: x: 2, y: 2, z: 4, core: 2. Of those that a mesh axis runs over, the one named last changes fastest.
Arguments:
- signal: bfloat16 [2, 2048, 1024], P('dp', 'sp'), may hold values from -6 to 6
- pace: float32 [2, 16], P('dp'), may hold values from 0.5 to 2
- log_step: float32 [64], P('sp'), may hold values from -5.52 to -4.42
- a_real: float32 [64, 64], P('sp'), may hold values from -4 to -0.002, as said below
- a_imag: float32 [64, 64], P('sp'), may hold values from 0.5 to 201.06177
- in_map: float32 [64, 2, 64, 16], P('sp'), may hold values from -3 to 3
- out_map: float32 [64, 2, 16, 64], P('sp'), may hold values from -0.5 to 0.5
- skip: float32 [1024], P('sp'), may hold values from -1 to 1
- init_state: float32 [2, 2, 64, 64], P('dp', None, 'sp'), may hold values from -5 to 5
- w_glu: bfloat16 [1024, 1024], P('sp', 'dp'), may hold values from -0.1875 to 0.1875
- b_glu: float32 [1024], replicated, may hold values from -4 to 4
- g_mix: float32 [1024], replicated, may hold values from 0.1 to 1.9
- w_out: bfloat16 [1024, 4096], P('sp', 'dp'), may hold values from -0.1875 to 0.1875
Outputs:
- result: bfloat16 [2, 2048, 4096], P('dp', 'sp')
Inputs may be any that keep to these rules, and one draw needn't show every extreme that they name: `a_real`: negative entries; within a group all entries are of one order.
All inputs are finite; a program needn't handle non-finite values.
Results may differ from a plain program's by a relative error of at most 0.0075.
Values may be sent and summed in bfloat16 or wider, within the bound.
A program may use at most 64 MiB of HBM per device.

v0:
```python
import functools
import math

import jax
import jax.numpy as jnp
from jax import lax
from jax.experimental import pallas as pl
from jax.experimental.pallas import tpu as pltpu
from jax.sharding import PartitionSpec as P

F32 = jnp.float32
BF16 = jnp.bfloat16
MESH = pl.DeviceIdType.MESH
LANES = 128
ORDERS = (("z", "y"),) * 5
CUTS = len(ORDERS) - 1


def spread_pieces(n_dp):
    return 2 if n_dp == 2 else 1


def cmul(ar, ai, br, bi):
    return ar * br - ai * bi, ar * bi + ai * br


def powers(br, bi, count):
    row = lax.broadcasted_iota(jnp.int32, (8, br.shape[1]), 0)
    pr = jnp.ones((8, br.shape[1]), F32)
    pi = jnp.zeros((8, br.shape[1]), F32)
    sr, si = br, bi
    for bit in (1, 2, 4):
        qr, qi = cmul(pr, pi, sr, si)
        on = (row & bit) != 0
        pr, pi = jnp.where(on, qr, pr), jnp.where(on, qi, pi)
        sr, si = cmul(sr, si, sr, si)
    size = 8
    while size < count:
        qr, qi = cmul(pr, pi, sr, si)
        pr = jnp.concatenate([pr, qr], axis=0)
        pi = jnp.concatenate([pi, qi], axis=0)
        sr, si = cmul(sr, si, sr, si)
        size *= 2
    return pr, pi


def gelu(v):
    return 0.5 * v * (1.0 + jnp.tanh(math.sqrt(2.0 / math.pi) * (v + 0.044715 * (v * v * v))))


def kernel(
    dims, sizes,
    sig, a_real, a_imag, init, in_map, out_map, log_step, pace, skip, b_glu, g_mix, wg_hbm, wo_hbm, out,
    buf0, buf1, buf2, buf3, buf4, mrx, ostage, tx, rx, atx, arx, bars, cmat,
    inm, lsem, wsend, wrecv, xsend, xrecv, asend, arecv, msend, mrecv, osend, orecv,
):
    n_sp, n_dp, tokens, wd, fold, rows, states = sizes
    spread = spread_pieces(n_dp)
    bufs = (buf0, buf1, buf2, buf3, buf4)
    me = lax.axis_index("sp")
    mx = lax.axis_index("dp")
    nc, ny, nz = dims["c"], dims["y"], dims["z"]
    at = {"x": mx, "c": lax.rem(me, nc), "y": lax.rem(me // nc, ny), "z": me // (nc * ny)}
    gcols = wg_hbm.shape[1]
    ocols = wo_hbm.shape[1] // CUTS

    def device(where):
        return {"sp": (where["z"] * ny + where["y"]) * nc + where["c"], "dp": where["x"]}

    def slot(t, where):
        index = (where["c"], where["z"], where["y"])
        return bufs[t].at[((where["x"],) if t < spread else ()) + index]

    local = [pltpu.make_async_copy(wg_hbm, slot(0, at), lsem.at[0])]
    for t in range(CUTS):
        local.append(pltpu.make_async_copy(
            wo_hbm.at[:, pl.ds(t * ocols, ocols)], slot(t + 1, at), lsem.at[t + 1]))
    for copy in local:
        copy.start()

    barrier = pltpu.get_barrier_semaphore()

    def greet(d, carry):
        pl.semaphore_signal(barrier, 1, device_id={"sp": lax.rem(me + d, n_sp), "dp": mx}, device_id_type=MESH)
        return carry

    lax.fori_loop(1, n_sp, greet, 0)
    for d in range(1, n_dp):
        pl.semaphore_signal(barrier, 1, device_id={"sp": me, "dp": lax.rem(mx + d, n_dp)}, device_id_type=MESH)

    part = lax.broadcasted_iota(jnp.int32, (rows, LANES), 1) // wd
    for tile in range(sig.shape[1] // LANES):
        pieces = [
            sig[p * rows:(p + 1) * rows, tile * LANES:(tile + 1) * LANES].astype(F32) for p in range(fold)
        ]
        for j in range(fold):
            acc = pieces[j]
            for p in range(fold):
                if p != j:
                    moved = pltpu.roll(pieces[p], ((p - j) * wd) % LANES, 1)
                    acc = jnp.where(part == p, moved, acc)
            tx[tile * fold + j] = acc.astype(BF16)

    pl.semaphore_wait(barrier, n_sp - 1 + n_dp - 1)

    def chunk_copy(src, dst, ssem, rsem, to, frm):
        return pltpu.make_async_remote_copy(
            src_ref=src, dst_ref=dst, send_sem=ssem.at[to], recv_sem=rsem.at[frm],
            device_id={"sp": to, "dp": mx}, device_id_type=MESH)

    def send_chunk(d, carry):
        to = lax.rem(me + d, n_sp)
        chunk_copy(tx.at[to], rx.at[me], xsend, xrecv, to, me).start()
        return carry

    lax.fori_loop(1, n_sp, send_chunk, 0)

    pending = []
    counter = [0]

    def guarded(cond, action):
        if cond is None:
            action()
        else:
            pl.when(cond)(action)

    def take():
        counter[0] += 1
        return counter[0] - 1

    def copy_of(k, ref, where):
        return pltpu.make_async_remote_copy(
            src_ref=ref, dst_ref=ref, send_sem=wsend.at[k], recv_sem=wrecv.at[k],
            device_id=device(where), device_id_type=MESH)

    def post(k, ref, where, cond=None):
        guarded(cond, lambda: copy_of(k, ref, where).start())
        pending.append((k, ref, where, cond))

    def arrive(k, ref, cond=None):
        guarded(cond, lambda: copy_of(k, ref, at).wait_recv())

    handed = {t: [] for t in range(len(ORDERS))}

    def sibling(t, where, cond):
        for d in range(1, nc):
            k = take()
            post(k, slot(t, where), dict(at, c=lax.rem(at["c"] + d, nc)), cond)
            handed[t].append((k, slot(t, dict(where, c=lax.rem(at["c"] + nc - d, nc))), cond))

    def source(move):
        where, cond = dict(at), None
        for axis, m in move.items():
            n, i = dims[axis], at[axis]
            if n == 2:
                where[axis] = 1 - i if m else i
            elif m:
                here = jnp.logical_and(i - m >= 0, i - m < n)
                cond = here if cond is None else jnp.logical_and(cond, here)
                where[axis] = jnp.clip(i - m, 0, n - 1)
        return where, cond

    def gather(t):
        order = ORDERS[t] + (("x",) if t < spread and n_dp == 2 else ())
        wave = [(None, {axis: 0 for axis in order}, 0)]
        while wave:
            later = []
            for k, move, level in wave:
                where, cond = source(move)
                if k is not None:
                    arrive(k, slot(t, where), cond)
                for deeper in range(level, len(order)):
                    axis = order[deeper]
                    n, i, m = dims[axis], at[axis], move[axis]
                    if n == 2:
                        ways = () if m else (1,)
                    else:
                        ways = (1, -1) if m == 0 else ((m // abs(m),) if abs(m) < n - 1 else ())
                    for way in ways:
                        k2 = take()
                        if n == 2:
                            to, ok = 1 - i, cond
                        else:
                            to, ok = jnp.clip(i + way, 0, n - 1), (i < n - 1) if way == 1 else (i > 0)
                            ok = ok if cond is None else jnp.logical_and(ok, cond)
                        post(k2, slot(t, where), dict(at, **{axis: to}), ok)
                        later.append((k2, dict(move, **{axis: m + way}), deeper))
                sibling(t, where, cond)
            wave = later
            yield
        for k, ref, cond in handed[t]:
            arrive(k, ref, cond)
        if t == 0 and n_dp > 2:
            swaps = []
            for d in range(1, n_dp):
                k = take()
                post(k, bufs[0].at[mx], dict(at, x=lax.rem(mx + d, n_dp)))
                swaps.append((k, lax.rem(mx + n_dp - d, n_dp)))
            yield
            for k, frm in swaps:
                arrive(k, bufs[0].at[frm])

    runs = {t: gather(t) for t in range(len(ORDERS))}

    def advance(which=None):
        for t in range(len(ORDERS)) if which is None else (which,):
            next(runs[t], None)

    def complete(t):
        for _ in runs[t]:
            pass

    for copy in local:
        copy.wait()
    advance()

    groups, entries = a_real.shape
    channels = wd // groups
    lane_group = lax.broadcasted_iota(jnp.int32, (1, states), 1) // entries
    block_row = lax.broadcasted_iota(jnp.int32, (n_sp, states), 0)

    def row_of(ref, *lead):
        found = [ref[lead + (slice(g, g + 1), slice(None))] for g in range(groups)]
        return jnp.concatenate(found, axis=1)

    a_re, a_im = row_of(a_real), row_of(a_imag)
    log_row = jnp.full((1, states), log_step[0], F32)
    for g in range(1, groups):
        log_row = jnp.where(lane_group == g, log_step[g], log_row)
    paces = jnp.full((n_sp, states), pace[0, 0], F32)
    for k in range(1, n_sp):
        paces = jnp.where(block_row == k, pace[0, k], paces)
    steps = paces * jnp.exp(log_row)

    def diagonal(blocks):
        lines = []
        for g in range(groups):
            line = [jnp.zeros((channels, entries), F32)] * groups
            line[g] = blocks[g]
            lines.append(jnp.concatenate(line, axis=1))
        return jnp.concatenate(lines, axis=0)

    for j in range(2):
        inm[j] = diagonal([in_map[g, j] for g in range(groups)])
    skips = jnp.concatenate([skip[...].reshape(1, wd)] * fold, axis=1)
    real, angle = a_re * steps, a_im * steps
    decay, growth = jnp.exp(real), jnp.exp(-real)
    cos, sin = jnp.cos(angle), jnp.sin(angle)
    bar_re, bar_im = decay * cos, decay * sin
    modulus = a_re * a_re + a_im * a_im
    bars[0] = bar_re
    bars[1] = bar_im
    bars[2] = growth * cos
    bars[3] = -growth * sin
    bars[4] = ((bar_re - 1.0) * a_re + bar_im * a_im) / modulus
    bars[5] = (bar_im * a_re - (bar_re - 1.0) * a_im) / modulus
    for p in range(fold):
        for j in range(2):
            blank = [jnp.zeros((wd, states), BF16)] * fold
            blank[p] = diagonal([out_map[g, j] for g in range(groups)]).astype(BF16)
            cmat[2 * p + j] = jnp.concatenate(blank, axis=0)

    rx[me] = tx[me]

    def take_chunk(d, carry):
        frm = lax.rem(me + n_sp - d, n_sp)
        chunk_copy(tx.at[me], rx.at[frm], xsend, xrecv, me, frm).wait_recv()
        return carry

    lax.fori_loop(1, n_sp, take_chunk, 0)

    span_row = lax.broadcasted_iota(jnp.int32, (tokens, tokens), 0)
    span_col = lax.broadcasted_iota(jnp.int32, (tokens, tokens), 1)
    tri = jnp.where(span_row >= span_col, 1.0, 0.0).astype(BF16)
    dot = functools.partial(jnp.dot, preferred_element_type=F32)

    def dot_t(a, b):
        return lax.dot_general(a, b, (((1,), (1,)), ((), ())), preferred_element_type=F32)

    def block(k, carry):
        before_re, before_im = carry
        br, bi, gr, gi, cr, ci = [bars[j, pl.ds(k, 1), :] for j in range(6)]
        chunk = rx[k]
        drive_re = (cr * inm[0] - ci * inm[1]).astype(BF16)
        drive_im = (cr * inm[1] + ci * inm[0]).astype(BF16)
        zero = jnp.zeros_like(drive_re)

        def inject(drive):
            return jnp.concatenate(
                [dot(chunk, jnp.concatenate([drive if q == p else zero for q in range(fold)], axis=0))
                 for p in range(fold)], axis=0)

        up_re, up_im = powers(gr, gi, tokens)
        sum_re, sum_im = cmul(inject(drive_re), inject(drive_im), up_re, up_im)
        sum_re, sum_im = dot(tri, sum_re.astype(BF16)), dot(tri, sum_im.astype(BF16))
        first_re, first_im = cmul(br, bi, before_re, before_im)
        down_re, down_im = powers(br, bi, tokens)
        state_re, state_im = cmul(sum_re + first_re, sum_im + first_im, down_re, down_im)
        s_re, s_im = state_re.astype(BF16), state_im.astype(BF16)
        response = skips * chunk.astype(F32)
        for p in range(fold):
            lines = slice(p * rows, (p + 1) * rows)
            response = response + dot_t(s_re[lines], cmat[2 * p]) - dot_t(s_im[lines], cmat[2 * p + 1])
        atx[k] = gelu(response).astype(BF16)

        @pl.when(k != me)
        def _():
            chunk_copy(atx.at[k], arx.at[me], asend, arecv, k, me).start()

        return state_re[tokens - 1:], state_im[tokens - 1:]

    carry = (row_of(init, 0, 0), row_of(init, 0, 1))
    advance()
    cuts = [n_sp * i // 2 for i in range(3)]
    for s in range(2):
        carry = lax.fori_loop(cuts[s], cuts[s + 1], block, carry)
        advance()

    arx[me] = atx[me]

    def take_act(d, carry):
        frm = lax.rem(me + n_sp - d, n_sp)
        chunk_copy(atx.at[me], arx.at[frm], asend, arecv, me, frm).wait_recv()
        return carry

    lax.fori_loop(1, n_sp, take_act, 0)
    tiles = []
    for tile in range(sig.shape[1] // LANES):
        chunks = [arx[tile * fold + j].astype(F32) for j in range(fold)]
        parts = []
        for p in range(fold):
            acc = chunks[p]
            for j in range(fold):
                if j != p:
                    moved = pltpu.roll(chunks[j], ((j - p) * wd) % LANES, 1)
                    acc = jnp.where(part == j, moved, acc)
            parts.append(acc)
        tiles.append(jnp.concatenate(parts, axis=0))
    act = jnp.concatenate(tiles, axis=1)
    act_bf = act.astype(BF16)

    def weight(t, x):
        found = []
        for i in range(n_sp):
            index = (i % nc, i // (nc * ny), (i // nc) % ny)
            found.append(bufs[t][((x,) if t < spread else ()) + index])
        return jnp.concatenate(found, axis=0)

    for step in range(2 * dims["z"]):
        advance()
    complete(0)
    gate = jnp.concatenate([dot(act_bf, weight(0, x)) for x in range(n_dp)], axis=1)
    gated = act * jax.nn.sigmoid(gate + b_glu[...].reshape(1, -1))
    scale = lax.rsqrt(jnp.mean(gated * gated, axis=-1, keepdims=True) + 1e-06)
    mixed = (gated * scale * g_mix[...].reshape(1, -1)).astype(BF16)
    mrx[mx] = mixed

    def mixed_copy(frm, to):
        return pltpu.make_async_remote_copy(
            src_ref=mrx.at[frm], dst_ref=mrx.at[frm], send_sem=msend.at[to], recv_sem=mrecv.at[frm],
            device_id={"sp": me, "dp": to}, device_id_type=MESH)

    others = [lax.rem(mx + d, n_dp) for d in range(1, n_dp)]
    for to in others:
        mixed_copy(mx, to).start()
    for t in range(1, spread):
        complete(t)
    for t in range(spread - 1):
        for x in range(n_dp):
            cols = slice((x * CUTS + t) * ocols, (x * CUTS + t + 1) * ocols)
            out[:, cols] = dot(mixed, weight(t + 1, x)).astype(BF16)
    for t in range(spread, CUTS + 1):
        complete(t)

    def out_copy(frm, to, t):
        cols = pl.ds(pl.multiple_of((frm * CUTS + t) * ocols, LANES), ocols)
        return pltpu.make_async_remote_copy(
            src_ref=ostage.at[to, t], dst_ref=out.at[:, cols], send_sem=osend.at[to, t],
            recv_sem=orecv.at[frm, t], device_id={"sp": me, "dp": to}, device_id_type=MESH)

    for to in others:
        mixed_copy(to, mx).wait_recv()
    alone = range(spread - 1, CUTS)
    for t in alone:
        for to in others:
            ostage[to, t] = dot(mrx[to], weight(t + 1, None)).astype(BF16)
            out_copy(mx, to, t).start()
    for t in alone:
        cols = pl.ds(pl.multiple_of((mx * CUTS + t) * ocols, LANES), ocols)
        out[:, cols] = dot(mixed, weight(t + 1, None)).astype(BF16)
    for t in alone:
        for frm in others:
            out_copy(frm, mx, t).wait_recv()
    for to in others:
        mixed_copy(mx, to).wait_send()
        for t in alone:
            out_copy(mx, to, t).wait_send()

    def drain(d, carry):
        to = lax.rem(me + d, n_sp)
        chunk_copy(tx.at[to], rx.at[me], xsend, xrecv, to, me).wait_send()
        chunk_copy(atx.at[to], arx.at[me], asend, arecv, to, me).wait_send()
        return carry

    lax.fori_loop(1, n_sp, drain, 0)
    for k, ref, where, cond in pending:
        guarded(cond, lambda: copy_of(k, ref, where).wait_send())


def per_device(
    signal, pace, log_step, a_real, a_imag, in_map, out_map, skip, init_state, w_glu, b_glu, g_mix, w_out
):
    n_sp, n_dp = lax.axis_size("sp"), lax.axis_size("dp")
    tokens, width = signal.shape[1], signal.shape[2]
    groups, entries = a_real.shape
    channels = width // (groups * n_sp)
    wd = groups * channels
    states = groups * entries
    fold = LANES // wd
    rows = tokens // fold
    assert signal.shape[0] == 1 and pace.shape[1] == n_sp and n_sp % 4 == 0
    dims = {"x": n_dp, "c": 2, "y": 2, "z": n_sp // 4}
    wrows = w_out.shape[0]
    gcols, ocols = w_glu.shape[1], w_out.shape[1] // CUTS
    copies = 2 * (len(ORDERS) + 3) * 2 * dims["z"] * dims["y"] + n_dp
    vmem = pl.BlockSpec(memory_space=pltpu.VMEM)
    smem = pl.BlockSpec(memory_space=pltpu.SMEM)
    hbm = pl.BlockSpec(memory_space=pl.ANY)
    chunk = pltpu.VMEM((n_sp, rows, LANES), BF16)
    sem = pltpu.SemaphoreType.DMA
    out_width = w_out.shape[1] * n_dp
    output = pl.pallas_call(
        functools.partial(kernel, dims, (n_sp, n_dp, tokens, wd, fold, rows, states)),
        out_shape=jax.ShapeDtypeStruct((tokens, out_width), BF16),
        in_specs=[vmem] * 6 + [smem] * 2 + [vmem] * 3 + [hbm] * 2,
        out_specs=vmem,
        scratch_shapes=[
            pltpu.VMEM(((n_dp,) if t < spread_pieces(n_dp) else ()) + (2, dims["z"], dims["y"], wrows, gcols if t == 0 else ocols), BF16)
            for t in range(len(ORDERS))
        ] + [
            pltpu.VMEM((n_dp, tokens, width), BF16),
            pltpu.VMEM((n_dp, CUTS, tokens, ocols), BF16),
        ] + [chunk] * 4 + [
            pltpu.VMEM((6, n_sp, states), F32),
            pltpu.VMEM((2 * fold, LANES, states), BF16),
            pltpu.VMEM((2, wd, states), F32),
            sem((8,)), sem((copies,)), sem((copies,)),
            sem((n_sp,)), sem((n_sp,)), sem((n_sp,)), sem((n_sp,)),
            sem((n_dp,)), sem((n_dp,)), sem((n_dp, CUTS)), sem((n_dp, CUTS)),
        ],
        compiler_params=pltpu.CompilerParams(
            collective_id=0, has_side_effects=True, vmem_limit_bytes=56 * 1024 * 1024),
    )(
        signal[0], a_real, a_imag, init_state, in_map.transpose(0, 1, 3, 2), out_map, log_step, pace, skip,
        b_glu, g_mix, w_glu, w_out)
    return output[None]


def solution(mesh):
    in_specs = (
        P("dp", "sp", None),
        P("dp", None),
        P("sp"),
        P("sp", None),
        P("sp", None),
        P("sp", None, None, None),
        P("sp", None, None, None),
        P("sp"),
        P("dp", None, "sp", None),
        P("sp", "dp"),
        P(),
        P(),
        P("sp", "dp"),
    )
    out_specs = P("dp", "sp", None)
    return jax.shard_map(
        per_device, mesh=mesh, in_specs=in_specs, out_specs=out_specs, check_vma=False
    )
```

profile of v0, /device:TPU:0, one launch (start us, length us, event | category | flops | bytes accessed | tf_op | source)
XLA Modules:
  0.0 72.1 jit_solution(1731680581570871639)
XLA Ops:
  0.0 69.8 %shard_map.127 = bf16[128,4096]{1,0:T(8,128)(2,1)} custom-call(bf16[128,1024]{1,0:T(8,128)(2,1)} %bitcast.4, f32[4,64]{1,0:T(4,128)} %a_real.1, f32[4,64]{1,0:T(4,128)} %a_imag.1, f32[1,2,4,64]{3,2,1,0:T(4,128)} %init.1, f32[4,2,16,64]{3,2,1,0:T(8,128)} %bitcast.5, f32[4,2,16,64]{3,2,1,0:T(8,128)} %out_map.1, f32[4]{0:T(128)} %log_step.1, f32[1,16]{1,0:T(1,128)} %pace.1, ...), custom_call_target="tpu_custom_call" | custom-call | tf_op jit(solution)/shard_map/pallas_call | solution.py:432
  69.8 2.3 %copy.15 = bf16[1,128,4096]{2,1,0:T(8,128)(2,1)} copy(bf16[1,128,4096]{2,1,0:T(8,128)(2,1)} %bitcast.3) | data formatting | bytes 2097152
where the time goes:
time: 73.2 us; the launch traced here: 72.1 us
  Pallas kernels  69.8 us (95%)
  local copies, waits for them, and re-layouts  2.29 us (3%)
    pallas_call x1, Pallas kernels, per_device(): pl.pallas_call(functools.partial(kernel, dims, (n_sp, n_dp, tokens, wd, f...  69.8 us
    unnamed x1, local copies, waits for them, and re-layouts  2.29 us

commit v1 on v0

v1 whole, which is shorter than its diff:
```python
import functools
import math

import jax
import jax.numpy as jnp
from jax import lax
from jax.experimental import pallas as pl
from jax.experimental.pallas import tpu as pltpu
from jax.sharding import PartitionSpec as P

F32 = jnp.float32
BF16 = jnp.bfloat16
MESH = pl.DeviceIdType.MESH
LANES = 128
ORDERS = (("z", "y", "x"), ("y", "z", "x"), ("x", "z", "y"), ("z", "y", "x"), ("z", "x", "y"))
CUTS = len(ORDERS) - 1
SHARE = 0.28
VMEM_LIMIT = 56 * 1024 * 1024


def cmul(ar, ai, br, bi):
    return ar * br - ai * bi, ar * bi + ai * br


def powers(br, bi, count):
    row = lax.broadcasted_iota(jnp.int32, (8, br.shape[1]), 0)
    pr = jnp.ones((8, br.shape[1]), F32)
    pi = jnp.zeros((8, br.shape[1]), F32)
    sr, si = br, bi
    for bit in (1, 2, 4):
        qr, qi = cmul(pr, pi, sr, si)
        on = (row & bit) != 0
        pr, pi = jnp.where(on, qr, pr), jnp.where(on, qi, pi)
        sr, si = cmul(sr, si, sr, si)
    size = 8
    while size < count:
        qr, qi = cmul(pr, pi, sr, si)
        pr = jnp.concatenate([pr, qr], axis=0)
        pi = jnp.concatenate([pi, qi], axis=0)
        sr, si = cmul(sr, si, sr, si)
        size *= 2
    return pr, pi


def gelu(v):
    return 0.5 * v * (1.0 + jnp.tanh(math.sqrt(2.0 / math.pi) * (v + 0.044715 * (v * v * v))))


def kernel(
    dims, sizes,
    sig_hbm, a_real_hbm, a_imag_hbm, init_hbm, in_map_hbm, out_map_hbm, log_hbm, pace_hbm, skip_hbm, b_glu_hbm,
    g_mix_hbm, wg_hbm, wo_hbm, out,
    buf0, buf1, buf2, buf3, buf4, sig, a_real, a_imag, init, in_map, out_map, log_step, pace, skip, b_glu, g_mix,
    tx, rx, atx, arx, bars, cmat, inm,
    lsem, isem, wsend, wrecv, ssend, srecv, xsend, xrecv, asend, arecv,
):
    n_sp, n_dp, tokens, wd, fold, rows, states = sizes
    bufs = (buf0, buf1, buf2, buf3, buf4)
    pieces = range(len(ORDERS))
    me = lax.axis_index("sp")
    mx = lax.axis_index("dp")
    nx, nc, ny, nz = dims["x"], dims["c"], dims["y"], dims["z"]
    paired = n_dp == 2
    half = nx * ny * nz
    at = {"x": mx, "c": lax.rem(me, nc), "y": lax.rem(me // nc, ny), "z": me // (nc * ny)}
    ocols = wo_hbm.shape[1] // CUTS

    def device(where):
        return {"sp": (where["z"] * ny + where["y"]) * nc + where["c"], "dp": where["x"]}

    def index(where):
        return (where["x"] * ny + where["y"]) * nz + where["z"]

    def slot(t, where):
        return bufs[t].at[where["c"] * half + index(where)]

    loads = [
        pltpu.make_async_copy(src, dst, isem.at[j]) for j, (src, dst) in enumerate((
            (sig_hbm, sig), (a_real_hbm, a_real), (a_imag_hbm, a_imag), (init_hbm, init), (in_map_hbm, in_map),
            (out_map_hbm, out_map), (log_hbm, log_step), (pace_hbm, pace), (skip_hbm, skip), (b_glu_hbm, b_glu),
            (g_mix_hbm, g_mix)))
    ]
    local = [pltpu.make_async_copy(wg_hbm, slot(0, at), lsem.at[0])]
    for t in range(CUTS):
        local.append(pltpu.make_async_copy(
            wo_hbm.at[:, pl.ds(t * ocols, ocols)], slot(t + 1, at), lsem.at[t + 1]))
    for copy in loads[:1] + local + loads[1:]:
        copy.start()

    barrier = pltpu.get_barrier_semaphore()

    def greet(d, carry):
        pl.semaphore_signal(barrier, 1, device_id={"sp": lax.rem(me + d, n_sp), "dp": mx}, device_id_type=MESH)
        return carry

    def greet_all(d, carry):
        to = lax.rem(me * n_dp + mx + d, n_sp * n_dp)
        pl.semaphore_signal(barrier, 1, device_id={"sp": to // n_dp, "dp": lax.rem(to, n_dp)}, device_id_type=MESH)
        return carry

    if paired:
        lax.fori_loop(1, n_sp, greet, 0)
        pl.semaphore_signal(barrier, 1, device_id={"sp": me, "dp": 1 - mx}, device_id_type=MESH)
        greeted = n_sp
    else:
        lax.fori_loop(1, n_sp * n_dp, greet_all, 0)
        greeted = n_sp * n_dp - 1

    loads[0].wait()
    part = lax.broadcasted_iota(jnp.int32, (rows, LANES), 1) // wd
    for tile in range(sig.shape[1] // LANES):
        cut = [
            sig[p * rows:(p + 1) * rows, tile * LANES:(tile + 1) * LANES].astype(F32) for p in range(fold)
        ]
        for j in range(fold):
            acc = cut[j]
            for p in range(fold):
                if p != j:
                    moved = pltpu.roll(cut[p], ((p - j) * wd) % LANES, 1)
                    acc = jnp.where(part == p, moved, acc)
            tx[tile * fold + j] = acc.astype(BF16)

    pl.semaphore_wait(barrier, greeted)

    def chunk_copy(src, dst, ssem, rsem, to):
        return pltpu.make_async_remote_copy(
            src_ref=src, dst_ref=dst, send_sem=ssem, recv_sem=rsem,
            device_id={"sp": to, "dp": mx}, device_id_type=MESH)

    def send_chunk(d, carry):
        to = lax.rem(me + d, n_sp)
        chunk_copy(tx.at[to], rx.at[me], xsend.at[0], xrecv.at[me], to).start()
        return carry

    lax.fori_loop(1, n_sp, send_chunk, 0)

    def guarded(cond, action):
        if cond is None:
            action()
        else:
            pl.when(cond)(action)

    def hop(t, where, to):
        return pltpu.make_async_remote_copy(
            src_ref=slot(t, where), dst_ref=slot(t, where), send_sem=wsend.at[t],
            recv_sem=wrecv.at[t, index(where)], device_id=device(to), device_id_type=MESH)

    def across(t, ref):
        return pltpu.make_async_remote_copy(
            src_ref=ref, dst_ref=ref, send_sem=ssend.at[t], recv_sem=srecv.at[t],
            device_id=device(dict(at, c=1 - at["c"])), device_id_type=MESH)

    def source(move):
        where, cond = dict(at), None
        for axis, m in move.items():
            n, i = dims[axis], at[axis]
            if n == 2:
                where[axis] = 1 - i if m else i
            elif m:
                here = jnp.logical_and(i - m >= 0, i - m < n)
                cond = here if cond is None else jnp.logical_and(cond, here)
                where[axis] = jnp.clip(i - m, 0, n - 1)
        return where, cond

    def onward(order, move, level):
        found = []
        for deeper in range(level, len(order)):
            axis = order[deeper]
            n, m = dims[axis], move[axis]
            if n == 2:
                ways = () if m else (1,)
            else:
                ways = (1, -1) if m == 0 else ((m // abs(m),) if abs(m) < n - 1 else ())
            found += [(axis, way, deeper) for way in ways]
        return found

    def forward(t, move, level, first=False):
        where, cond = source(move)

        def act():
            if not first:
                hop(t, where, at).wait_recv()
            for axis, way, _ in onward(ORDERS[t], move, level):
                n, i = dims[axis], at[axis]
                if n == 2:
                    hop(t, where, dict(at, **{axis: 1 - i})).start()
                else:
                    ok = (i < n - 1) if way == 1 else (i > 0)
                    to = dict(at, **{axis: jnp.clip(i + way, 0, n - 1)})
                    pl.when(ok)(lambda to=to: hop(t, where, to).start())
            across(t, slot(t, where)).start()

        guarded(cond, act)

    def sends(t, z):
        total, wave = 0, [({axis: 0 for axis in ORDERS[t]}, 0)]
        while wave:
            later = []
            for move, level in wave:
                valid = 0 <= z - move["z"] < nz
                for axis, way, deeper in onward(ORDERS[t], move, level):
                    total += valid and (axis != "z" or 0 <= z + way < nz)
                    later.append((dict(move, **{axis: move[axis] + way}), deeper))
            wave = later
        return total

    def plan():
        waves, current = [], [(t, {axis: 0 for axis in ORDERS[t]}, 0) for t in pieces]
        while current:
            later = []
            for t, move, level in current:
                for axis, way, deeper in onward(ORDERS[t], move, level):
                    later.append((t, dict(move, **{axis: move[axis] + way}), deeper))
            waves += later
            current = later
        return waves

    def toss(t, d):
        to = lax.rem(me * n_dp + mx + d, n_sp * n_dp)
        return pltpu.make_async_remote_copy(
            src_ref=slot(t, at), dst_ref=slot(t, at), send_sem=wsend.at[t], recv_sem=wrecv.at[t, 0],
            device_id={"sp": to // n_dp, "dp": lax.rem(to, n_dp)}, device_id_type=MESH)

    for copy in local:
        copy.wait()
    events = []
    if paired:
        events = plan()
        for t in pieces:
            forward(t, {axis: 0 for axis in ORDERS[t]}, 0, True)
    else:
        for t in pieces:
            def toss_one(d, carry, t=t):
                toss(t, d).start()
                return carry

            lax.fori_loop(1, n_sp * n_dp, toss_one, 0)

    for copy in loads[1:]:
        copy.wait()
    groups, entries = a_real.shape
    channels = wd // groups
    lane_group = lax.broadcasted_iota(jnp.int32, (1, states), 1) // entries

    def row_of(ref, *lead):
        found = [ref[lead + (slice(g, g + 1), slice(None))] for g in range(groups)]
        return jnp.concatenate(found, axis=1)

    a_re, a_im = row_of(a_real), row_of(a_imag)
    logs = log_step[...]
    log_row = jnp.broadcast_to(logs[:, :1], (1, states))
    for g in range(1, groups):
        log_row = jnp.where(lane_group == g, jnp.broadcast_to(logs[:, g:g + 1], (1, states)), log_row)
    on = lax.broadcasted_iota(jnp.int32, (n_sp, n_sp), 0) == lax.broadcasted_iota(jnp.int32, (n_sp, n_sp), 1)
    paces = jnp.sum(jnp.where(on, jnp.broadcast_to(pace[...], (n_sp, n_sp)), 0.0), axis=1, keepdims=True)
    steps = paces * jnp.exp(log_row)

    def diagonal(blocks):
        lines = []
        for g in range(groups):
            line = [jnp.zeros((channels, entries), F32)] * groups
            line[g] = blocks[g]
            lines.append(jnp.concatenate(line, axis=1))
        return jnp.concatenate(lines, axis=0)

    for j in range(2):
        inm[j] = diagonal([in_map[g, j] for g in range(groups)])
    skips = jnp.concatenate([skip[...]] * fold, axis=1)
    real, angle = a_re * steps, a_im * steps
    decay, growth = jnp.exp(real), jnp.exp(-real)
    cos, sin = jnp.cos(angle), jnp.sin(angle)
    bar_re, bar_im = decay * cos, decay * sin
    modulus = a_re * a_re + a_im * a_im
    bars[0] = bar_re
    bars[1] = bar_im
    bars[2] = growth * cos
    bars[3] = -growth * sin
    bars[4] = ((bar_re - 1.0) * a_re + bar_im * a_im) / modulus
    bars[5] = (bar_im * a_re - (bar_re - 1.0) * a_im) / modulus
    for p in range(fold):
        for j in range(2):
            blank = [jnp.zeros((wd, states), BF16)] * fold
            blank[p] = diagonal([out_map[g, j] for g in range(groups)]).astype(BF16)
            cmat[2 * p + j] = jnp.concatenate(blank, axis=0)

    rx[me] = tx[me]

    span_row = lax.broadcasted_iota(jnp.int32, (tokens, tokens), 0)
    span_col = lax.broadcasted_iota(jnp.int32, (tokens, tokens), 1)
    tri = jnp.where(span_row >= span_col, 1.0, 0.0).astype(BF16)
    dot = functools.partial(jnp.dot, preferred_element_type=F32)

    def dot_t(a, b):
        return lax.dot_general(a, b, (((1,), (1,)), ((), ())), preferred_element_type=F32)

    inside = int(len(events) * SHARE)
    cuts = [inside * k // n_sp for k in range(n_sp + 1)]

    def block(k, carry):
        for i in range(n_sp):
            if cuts[i] < cuts[i + 1]:
                @pl.when(k == i)
                def _():
                    for event in events[cuts[i]:cuts[i + 1]]:
                        forward(*event)

        @pl.when(k != me)
        def _():
            chunk_copy(tx.at[me], rx.at[k], xsend.at[0], xrecv.at[k], me).wait_recv()

        before_re, before_im = carry
        br, bi, gr, gi, cr, ci = [bars[j, pl.ds(k, 1), :] for j in range(6)]
        chunk = rx[k]
        drive_re = (cr * inm[0] - ci * inm[1]).astype(BF16)
        drive_im = (cr * inm[1] + ci * inm[0]).astype(BF16)
        zero = jnp.zeros_like(drive_re)

        def inject(drive):
            return jnp.concatenate(
                [dot(chunk, jnp.concatenate([drive if q == p else zero for q in range(fold)], axis=0))
                 for p in range(fold)], axis=0)

        up_re, up_im = powers(gr, gi, tokens)
        sum_re, sum_im = cmul(inject(drive_re), inject(drive_im), up_re, up_im)
        sum_re, sum_im = dot(tri, sum_re.astype(BF16)), dot(tri, sum_im.astype(BF16))
        first_re, first_im = cmul(br, bi, before_re, before_im)
        down_re, down_im = powers(br, bi, tokens)
        state_re, state_im = cmul(sum_re + first_re, sum_im + first_im, down_re, down_im)
        s_re, s_im = state_re.astype(BF16), state_im.astype(BF16)
        response = skips * chunk.astype(F32)
        for p in range(fold):
            lines = slice(p * rows, (p + 1) * rows)
            response = response + dot_t(s_re[lines], cmat[2 * p]) - dot_t(s_im[lines], cmat[2 * p + 1])
        atx[k] = gelu(response).astype(BF16)

        @pl.when(k != me)
        def _():
            chunk_copy(atx.at[k], arx.at[me], asend.at[0], arecv.at[0], k).start()

        return state_re[tokens - 1:], state_im[tokens - 1:]

    lax.fori_loop(0, n_sp, block, (row_of(init, 0, 0), row_of(init, 0, 1)))

    arx[me] = atx[me]
    most = n_sp - 1
    chunk_copy(atx.at[pl.ds(0, most)], arx.at[pl.ds(0, most)], asend.at[0], arecv.at[0], me).wait_recv()
    tiles = []
    for tile in range(sig.shape[1] // LANES):
        chunks = [arx[tile * fold + j].astype(F32) for j in range(fold)]
        parts = []
        for p in range(fold):
            acc = chunks[p]
            for j in range(fold):
                if j != p:
                    moved = pltpu.roll(chunks[j], ((j - p) * wd) % LANES, 1)
                    acc = jnp.where(part == j, moved, acc)
            parts.append(acc)
        tiles.append(jnp.concatenate(parts, axis=0))
    act = jnp.concatenate(tiles, axis=1)
    act_bf = act.astype(BF16)

    def weight(t, x):
        found = []
        for i in range(n_sp):
            where = {"x": x, "c": i % nc, "z": i // (nc * ny), "y": (i // nc) % ny}
            found.append(bufs[t][where["c"] * half + index(where)])
        return jnp.concatenate(found, axis=0)

    rest = events[inside:]
    for event in rest:
        forward(*event)

    def complete(t):
        if paired:
            across(t, bufs[t].at[pl.ds((1 - at["c"]) * half, half)]).wait_recv()
        else:
            every = bufs[t].at[pl.ds(0, n_sp * n_dp - 1)]
            pltpu.make_async_remote_copy(
                src_ref=every, dst_ref=every, send_sem=wsend.at[t], recv_sem=wrecv.at[t, 0],
                device_id=device(at), device_id_type=MESH).wait_recv()

    complete(0)
    gate = jnp.concatenate([dot(act_bf, weight(0, x)) for x in range(n_dp)], axis=1)
    gated = act * jax.nn.sigmoid(gate + b_glu[...])
    scale = lax.rsqrt(jnp.mean(gated * gated, axis=-1, keepdims=True) + 1e-06)
    mixed = (gated * scale * g_mix[...]).astype(BF16)

    for t in range(1, CUTS + 1):
        complete(t)
        for x in range(n_dp):
            cols = slice((x * CUTS + t - 1) * ocols, (x * CUTS + t) * ocols)
            out[:, cols] = dot(mixed, weight(t, x)).astype(BF16)

    chunk_copy(tx.at[pl.ds(0, most)], rx.at[pl.ds(0, most)], xsend.at[0], xrecv.at[0], me).wait_send()
    chunk_copy(atx.at[pl.ds(0, most)], arx.at[pl.ds(0, most)], asend.at[0], arecv.at[0], me).wait_send()

    def drained(t, count):
        sent = bufs[t].at[pl.ds(0, count)]
        pltpu.make_async_remote_copy(
            src_ref=sent, dst_ref=sent, send_sem=wsend.at[t], recv_sem=wrecv.at[t, 0],
            device_id=device(at), device_id_type=MESH).wait_send()

    for t in pieces:
        if paired:
            across(t, bufs[t].at[pl.ds(at["c"] * half, half)]).wait_send()
            for z in range(nz):
                pl.when(at["z"] == z)(lambda z=z: drained(t, sends(t, z)))
        else:
            drained(t, n_sp * n_dp - 1)


def per_device(
    signal, pace, log_step, a_real, a_imag, in_map, out_map, skip, init_state, w_glu, b_glu, g_mix, w_out
):
    n_sp, n_dp = lax.axis_size("sp"), lax.axis_size("dp")
    tokens, width = signal.shape[1], signal.shape[2]
    groups, entries = a_real.shape
    channels = width // (groups * n_sp)
    wd = groups * channels
    states = groups * entries
    fold = LANES // wd
    rows = tokens // fold
    assert signal.shape[0] == 1 and pace.shape[1] == n_sp and n_sp % 4 == 0
    dims = {"x": n_dp, "c": 2, "y": 2, "z": n_sp // 4}
    wrows = w_out.shape[0]
    gcols, ocols = w_glu.shape[1], w_out.shape[1] // CUTS
    slots = n_sp * n_dp
    marks = slots // 2 if n_dp == 2 else 1
    chunk = pltpu.VMEM((n_sp, rows, LANES), BF16)
    sem = pltpu.SemaphoreType.DMA
    operands = (
        signal[0], a_real, a_imag, init_state, in_map.transpose(0, 1, 3, 2), out_map, log_step.reshape(1, -1), pace,
        skip.reshape(1, -1), b_glu.reshape(1, -1), g_mix.reshape(1, -1))
    output = pl.pallas_call(
        functools.partial(kernel, dims, (n_sp, n_dp, tokens, wd, fold, rows, states)),
        out_shape=pltpu.VMEM((tokens, w_out.shape[1] * n_dp), BF16),
        in_specs=[pl.BlockSpec(memory_space=pltpu.HBM)] * (len(operands) + 2),
        out_specs=pl.BlockSpec(memory_space=pltpu.VMEM),
        scratch_shapes=[
            pltpu.VMEM((slots, wrows, gcols if t == 0 else ocols), BF16) for t in range(len(ORDERS))
        ] + [pltpu.VMEM(x.shape, x.dtype) for x in operands] + [chunk] * 4 + [
            pltpu.VMEM((6, n_sp, states), F32),
            pltpu.VMEM((2 * fold, LANES, states), BF16),
            pltpu.VMEM((2, wd, states), F32),
            sem((len(ORDERS),)), sem((len(operands),)),
            sem((len(ORDERS),)), sem((len(ORDERS), marks)), sem((len(ORDERS),)), sem((len(ORDERS),)),
            sem((1,)), sem((n_sp,)), sem((1,)), sem((1,)),
        ],
        compiler_params=pltpu.CompilerParams(
            collective_id=0, has_side_effects=True, vmem_limit_bytes=VMEM_LIMIT),
    )(*operands, w_glu, w_out)
    return output[None]


def solution(mesh):
    in_specs = (
        P("dp", "sp", None),
        P("dp", None),
        P("sp"),
        P("sp", None),
        P("sp", None),
        P("sp", None, None, None),
        P("sp", None, None, None),
        P("sp"),
        P("dp", None, "sp", None),
        P("sp", "dp"),
        P(),
        P(),
        P("sp", "dp"),
    )
    out_specs = P("dp", "sp", None)
    return jax.shard_map(
        per_device, mesh=mesh, in_specs=in_specs, out_specs=out_specs, check_vma=False
    )
```

time: 73.2 us -> 60.8 us (0.83)
  the two profiles are of different devices: /device:TPU:0 before, /device:TPU:29 now
where the time goes in v1:
time: 60.8 us; the launch traced here: 60.6 us
  Pallas kernels  59.7 us (98%)
  local copies, waits for them, and re-layouts  0.97 us (2%)
    pallas_call x1, Pallas kernels, per_device(): pl.pallas_call(functools.partial(kernel, dims, (n_sp, n_dp, tokens, wd, f...  59.7 us

profile of v1, /device:TPU:29, one launch (start us, length us, event | category | flops | bytes accessed | tf_op | source)
XLA Modules:
  0.0 60.6 jit_solution(2626276044765243905)
XLA Ops:
  0.0 59.7 %shard_map.127 = bf16[128,4096]{1,0:T(8,128)(2,1)S(1)} custom-call(bf16[128,1024]{1,0:T(8,128)(2,1)} %bitcast.8, f32[4,64]{1,0:T(4,128)} %a_real_hbm.1, f32[4,64]{1,0:T(4,128)} %a_imag_hbm.1, f32[1,2,4,64]{3,2,1,0:T(4,128)} %init_hbm.1, f32[4,2,16,64]{3,2,1,0:T(8,128)} %bitcast.9, f32[4,2,16,64]{3,2,1,0:T(8,128)} %out_map_hbm.1, f32[1,4]{1,0:T(1,128)} %bitcast.12, ...), custom_call_target="tpu_custom_call" | custom-call | tf_op jit(solution)/shard_map/pallas_call | solution.py:434
  59.7 1.0 %copy.15 = bf16[1,128,4096]{2,1,0:T(8,128)(2,1)} copy(bf16[1,128,4096]{2,1,0:T(8,128)(2,1)S(1)} %bitcast.7) | data formatting | bytes 2097152

commit v2 on v1

--- a/solution.py
+++ b/solution.py
@@ -12,9 +12,11 @@
 BF16 = jnp.bfloat16
 MESH = pl.DeviceIdType.MESH
 LANES = 128
-ORDERS = (("z", "y", "x"), ("y", "z", "x"), ("x", "z", "y"), ("z", "y", "x"), ("z", "x", "y"))
+ORDERS = (("z", "y", "x"), ("z", "y", "x"), ("x", "z", "y"), ("y", "z", "x"), ("z", "x", "y"))
 CUTS = len(ORDERS) - 1
-SHARE = 0.28
+SHARE = 0.35
+LAG = 0.2
+AHEAD = 2
 VMEM_LIMIT = 56 * 1024 * 1024
 
 
@@ -84,8 +86,6 @@
     for t in range(CUTS):
         local.append(pltpu.make_async_copy(
             wo_hbm.at[:, pl.ds(t * ocols, ocols)], slot(t + 1, at), lsem.at[t + 1]))
-    for copy in loads[:1] + local + loads[1:]:
-        copy.start()
 
     barrier = pltpu.get_barrier_semaphore()
 
@@ -106,6 +106,8 @@
         lax.fori_loop(1, n_sp * n_dp, greet_all, 0)
         greeted = n_sp * n_dp - 1
 
+    for copy in loads[:1] + local + loads[1:]:
+        copy.start()
     loads[0].wait()
     part = lax.broadcasted_iota(jnp.int32, (rows, LANES), 1) // wd
     for tile in range(sig.shape[1] // LANES):
@@ -206,14 +208,15 @@
 
     def plan():
         waves, current = [], [(t, {axis: 0 for axis in ORDERS[t]}, 0) for t in pieces]
+        depth = 0
         while current:
             later = []
             for t, move, level in current:
                 for axis, way, deeper in onward(ORDERS[t], move, level):
                     later.append((t, dict(move, **{axis: move[axis] + way}), deeper))
-            waves += later
-            current = later
-        return waves
+            waves += [(depth + LAG * event[0], event) for event in later]
+            current, depth = later, depth + 1
+        return [event for _, event in sorted(waves, key=lambda found: found[0])]
 
     def toss(t, d):
         to = lax.rem(me * n_dp + mx + d, n_sp * n_dp)
@@ -341,23 +344,7 @@
 
     lax.fori_loop(0, n_sp, block, (row_of(init, 0, 0), row_of(init, 0, 1)))
 
-    arx[me] = atx[me]
     most = n_sp - 1
-    chunk_copy(atx.at[pl.ds(0, most)], arx.at[pl.ds(0, most)], asend.at[0], arecv.at[0], me).wait_recv()
-    tiles = []
-    for tile in range(sig.shape[1] // LANES):
-        chunks = [arx[tile * fold + j].astype(F32) for j in range(fold)]
-        parts = []
-        for p in range(fold):
-            acc = chunks[p]
-            for j in range(fold):
-                if j != p:
-                    moved = pltpu.roll(chunks[j], ((j - p) * wd) % LANES, 1)
-                    acc = jnp.where(part == j, moved, acc)
-            parts.append(acc)
-        tiles.append(jnp.concatenate(parts, axis=0))
-    act = jnp.concatenate(tiles, axis=1)
-    act_bf = act.astype(BF16)
 
     def weight(t, x):
         found = []
@@ -365,10 +352,6 @@
             where = {"x": x, "c": i % nc, "z": i // (nc * ny), "y": (i // nc) % ny}
             found.append(bufs[t][where["c"] * half + index(where)])
         return jnp.concatenate(found, axis=0)
-
-    rest = events[inside:]
-    for event in rest:
-        forward(*event)
 
     def complete(t):
         if paired:
@@ -379,17 +362,43 @@
                 src_ref=every, dst_ref=every, send_sem=wsend.at[t], recv_sem=wrecv.at[t, 0],
                 device_id=device(at), device_id_type=MESH).wait_recv()
 
-    complete(0)
-    gate = jnp.concatenate([dot(act_bf, weight(0, x)) for x in range(n_dp)], axis=1)
-    gated = act * jax.nn.sigmoid(gate + b_glu[...])
-    scale = lax.rsqrt(jnp.mean(gated * gated, axis=-1, keepdims=True) + 1e-06)
-    mixed = (gated * scale * g_mix[...]).astype(BF16)
-
-    for t in range(1, CUTS + 1):
-        complete(t)
-        for x in range(n_dp):
-            cols = slice((x * CUTS + t - 1) * ocols, (x * CUTS + t) * ocols)
-            out[:, cols] = dot(mixed, weight(t, x)).astype(BF16)
+    def activated():
+        arx[me] = atx[me]
+        chunk_copy(atx.at[pl.ds(0, most)], arx.at[pl.ds(0, most)], asend.at[0], arecv.at[0], me).wait_recv()
+        tiles = []
+        for tile in range(sig.shape[1] // LANES):
+            chunks = [arx[tile * fold + j].astype(F32) for j in range(fold)]
+            parts = []
+            for p in range(fold):
+                acc = chunks[p]
+                for j in range(fold):
+                    if j != p:
+                        moved = pltpu.roll(chunks[j], ((j - p) * wd) % LANES, 1)
+                        acc = jnp.where(part == j, moved, acc)
+                parts.append(acc)
+            tiles.append(jnp.concatenate(parts, axis=0))
+        return jnp.concatenate(tiles, axis=1)
+
+    rest = events[inside:]
+    mixed = None
+    for t in pieces:
+        soon = t if t == 0 else t + AHEAD
+        last = max((i for i, event in enumerate(rest) if event[0] <= soon), default=-1)
+        for event in rest[:last + 1]:
+            forward(*event)
+        rest = rest[last + 1:]
+        if t == 0:
+            act = activated()
+            complete(0)
+            gate = jnp.concatenate([dot(act.astype(BF16), weight(0, x)) for x in range(n_dp)], axis=1)
+            gated = act * jax.nn.sigmoid(gate + b_glu[...])
+            scale = lax.rsqrt(jnp.mean(gated * gated, axis=-1, keepdims=True) + 1e-06)
+            mixed = (gated * scale * g_mix[...]).astype(BF16)
+        else:
+            complete(t)
+            for x in range(n_dp):
+                cols = slice((x * CUTS + t - 1) * ocols, (x * CUTS + t) * ocols)
+                out[:, cols] = dot(mixed, weight(t, x)).astype(BF16)
 
     chunk_copy(tx.at[pl.ds(0, most)], rx.at[pl.ds(0, most)], xsend.at[0], xrecv.at[0], me).wait_send()
     chunk_copy(atx.at[pl.ds(0, most)], arx.at[pl.ds(0, most)], asend.at[0], arecv.at[0], me).wait_send()

time: 60.8 us -> 55.3 us (0.910)
  the two profiles are of different devices: /device:TPU:29 before, /device:TPU:0 now
where the time goes in v2:
time: 55.3 us; the launch traced here: 55.2 us
  Pallas kernels  54.2 us (98%)
  local copies, waits for them, and re-layouts  0.97 us (2%)
    pallas_call x1, Pallas kernels, per_device(): pl.pallas_call(functools.partial(kernel, dims, (n_sp, n_dp, tokens, wd, f...  54.2 us

profile of v2, /device:TPU:0, one launch (start us, length us, event | category | flops | bytes accessed | tf_op | source)
XLA Modules:
  0.0 55.2 jit_solution(1837777952808457465)
XLA Ops:
  0.0 54.2 %shard_map.127 = bf16[128,4096]{1,0:T(8,128)(2,1)S(1)} custom-call(bf16[128,1024]{1,0:T(8,128)(2,1)} %bitcast.8, f32[4,64]{1,0:T(4,128)} %a_real_hbm.1, f32[4,64]{1,0:T(4,128)} %a_imag_hbm.1, f32[1,2,4,64]{3,2,1,0:T(4,128)} %init_hbm.1, f32[4,2,16,64]{3,2,1,0:T(8,128)} %bitcast.9, f32[4,2,16,64]{3,2,1,0:T(8,128)} %out_map_hbm.1, f32[1,4]{1,0:T(1,128)} %bitcast.12, ...), custom_call_target="tpu_custom_call" | custom-call | tf_op jit(solution)/shard_map/pallas_call | solution.py:443
  54.2 1.0 %copy.15 = bf16[1,128,4096]{2,1,0:T(8,128)(2,1)} copy(bf16[1,128,4096]{2,1,0:T(8,128)(2,1)S(1)} %bitcast.7) | data formatting | bytes 2097152

commit v3 on v2

--- a/solution.py
+++ b/solution.py
@@ -14,9 +14,10 @@
 LANES = 128
 ORDERS = (("z", "y", "x"), ("z", "y", "x"), ("x", "z", "y"), ("y", "z", "x"), ("z", "x", "y"))
 CUTS = len(ORDERS) - 1
-SHARE = 0.35
-LAG = 0.2
-AHEAD = 2
+SHARE = 0.5
+PRE = 0.14
+LAGS = (0.0, 0.2, 0.4, 0.6, 0.8)
+AHEAD = 3
 VMEM_LIMIT = 56 * 1024 * 1024
 
 
@@ -54,7 +55,7 @@
     g_mix_hbm, wg_hbm, wo_hbm, out,
     buf0, buf1, buf2, buf3, buf4, sig, a_real, a_imag, init, in_map, out_map, log_step, pace, skip, b_glu, g_mix,
     tx, rx, atx, arx, bars, cmat, inm,
-    lsem, isem, wsend, wrecv, ssend, srecv, xsend, xrecv, asend, arecv,
+    ready, lsem, isem, wsend, wrecv, ssend, srecv, xsend, xrecv, asend, arecv,
 ):
     n_sp, n_dp, tokens, wd, fold, rows, states = sizes
     bufs = (buf0, buf1, buf2, buf3, buf4)
@@ -89,9 +90,26 @@
 
     barrier = pltpu.get_barrier_semaphore()
 
-    def greet(d, carry):
-        pl.semaphore_signal(barrier, 1, device_id={"sp": lax.rem(me + d, n_sp), "dp": mx}, device_id_type=MESH)
-        return carry
+    def guarded(cond, action):
+        if cond is None:
+            action()
+        else:
+            pl.when(cond)(action)
+
+    def step(axis, way):
+        n, i = dims[axis], at[axis]
+        if n == 2:
+            return dict(at, **{axis: 1 - i}), None
+        return dict(at, **{axis: jnp.clip(i + way, 0, n - 1)}), (i < n - 1) if way == 1 else (i > 0)
+
+    ways = [(axis, way) for axis in ("z", "y", "x", "c") for way in ((1,) if dims[axis] == 2 else (1, -1))]
+
+    def tell(semaphore, axis, way):
+        to, ok = step(axis, way)
+        guarded(ok, lambda: pl.semaphore_signal(semaphore, 1, device_id=device(to), device_id_type=MESH))
+
+    def hear(semaphore, axis, way):
+        guarded(step(axis, way)[1], lambda: pl.semaphore_wait(semaphore, 1))
 
     def greet_all(d, carry):
         to = lax.rem(me * n_dp + mx + d, n_sp * n_dp)
@@ -99,15 +117,116 @@
         return carry
 
     if paired:
-        lax.fori_loop(1, n_sp, greet, 0)
-        pl.semaphore_signal(barrier, 1, device_id={"sp": me, "dp": 1 - mx}, device_id_type=MESH)
-        greeted = n_sp
+        for axis, way in ways:
+            tell(barrier, axis, way)
     else:
         lax.fori_loop(1, n_sp * n_dp, greet_all, 0)
-        greeted = n_sp * n_dp - 1
 
     for copy in loads[:1] + local + loads[1:]:
         copy.start()
+    if paired:
+        peers = [step(axis, way)[1] for axis, way in ways]
+        pl.semaphore_wait(barrier, sum(1 if ok is None else jnp.where(ok, 1, 0) for ok in peers))
+    else:
+        pl.semaphore_wait(barrier, n_sp * n_dp - 1)
+
+    def hop(t, where, to):
+        return pltpu.make_async_remote_copy(
+            src_ref=slot(t, where), dst_ref=slot(t, where), send_sem=wsend.at[t],
+            recv_sem=wrecv.at[t, index(where)], device_id=device(to), device_id_type=MESH)
+
+    def across(t, ref):
+        return pltpu.make_async_remote_copy(
+            src_ref=ref, dst_ref=ref, send_sem=ssend.at[t], recv_sem=srecv.at[t],
+            device_id=device(dict(at, c=1 - at["c"])), device_id_type=MESH)
+
+    def source(move):
+        where, cond = dict(at), None
+        for axis, m in move.items():
+            n, i = dims[axis], at[axis]
+            if n == 2:
+                where[axis] = 1 - i if m else i
+            elif m:
+                here = jnp.logical_and(i - m >= 0, i - m < n)
+                cond = here if cond is None else jnp.logical_and(cond, here)
+                where[axis] = jnp.clip(i - m, 0, n - 1)
+        return where, cond
+
+    def onward(order, move, level):
+        found = []
+        for deeper in range(level, len(order)):
+            axis = order[deeper]
+            n, m = dims[axis], move[axis]
+            if n == 2:
+                ways = () if m else (1,)
+            else:
+                ways = (1, -1) if m == 0 else ((m // abs(m),) if abs(m) < n - 1 else ())
+            found += [(axis, way, deeper) for way in ways]
+        return found
+
+    def forward(t, move, level, first=False):
+        where, cond = source(move)
+
+        def act():
+            if not first:
+                hop(t, where, at).wait_recv()
+            for axis, way, _ in onward(ORDERS[t], move, level):
+                n, i = dims[axis], at[axis]
+                if n == 2:
+                    hop(t, where, dict(at, **{axis: 1 - i})).start()
+                else:
+                    ok = (i < n - 1) if way == 1 else (i > 0)
+                    to = dict(at, **{axis: jnp.clip(i + way, 0, n - 1)})
+                    pl.when(ok)(lambda to=to: hop(t, where, to).start())
+            across(t, slot(t, where)).start()
+
+        guarded(cond, act)
+
+    def sends(t, z):
+        total, wave = 0, [({axis: 0 for axis in ORDERS[t]}, 0)]
+        while wave:
+            later = []
+            for move, level in wave:
+                valid = 0 <= z - move["z"] < nz
+                for axis, way, deeper in onward(ORDERS[t], move, level):
+                    total += valid and (axis != "z" or 0 <= z + way < nz)
+                    later.append((dict(move, **{axis: move[axis] + way}), deeper))
+            wave = later
+        return total
+
+    def plan():
+        waves, current = [], [(t, {axis: 0 for axis in ORDERS[t]}, 0) for t in pieces]
+        depth = 0
+        while current:
+            later = []
+            for t, move, level in current:
+                for axis, way, deeper in onward(ORDERS[t], move, level):
+                    later.append((t, dict(move, **{axis: move[axis] + way}), deeper))
+            waves += [(depth + LAGS[event[0]], event) for event in later]
+            current, depth = later, depth + 1
+        return [event for _, event in sorted(waves, key=lambda found: found[0])]
+
+    def toss(t, d):
+        to = lax.rem(me * n_dp + mx + d, n_sp * n_dp)
+        return pltpu.make_async_remote_copy(
+            src_ref=slot(t, at), dst_ref=slot(t, at), send_sem=wsend.at[t], recv_sem=wrecv.at[t, 0],
+            device_id={"sp": to // n_dp, "dp": lax.rem(to, n_dp)}, device_id_type=MESH)
+
+    for copy in local:
+        copy.wait()
+    events = []
+    if paired:
+        events = plan()
+        for t in pieces:
+            forward(t, {axis: 0 for axis in ORDERS[t]}, 0, True)
+    else:
+        for t in pieces:
+            def toss_one(d, carry, t=t):
+                toss(t, d).start()
+                return carry
+
+            lax.fori_loop(1, n_sp * n_dp, toss_one, 0)
+
     loads[0].wait()
     part = lax.broadcasted_iota(jnp.int32, (rows, LANES), 1) // wd
     for tile in range(sig.shape[1] // LANES):
@@ -122,7 +241,17 @@
                     acc = jnp.where(part == p, moved, acc)
             tx[tile * fold + j] = acc.astype(BF16)
 
-    pl.semaphore_wait(barrier, greeted)
+    if paired:
+        if dims["z"] > 2:
+            for way in (1, -1):
+                hear(ready.at[0 if way == 1 else 1], "z", -way)
+                tell(ready.at[0 if way == 1 else 1], "z", way)
+        else:
+            tell(ready.at[0], "z", 1)
+            hear(ready.at[0], "z", 1)
+        for j, axis in ((2, "y"), (3, "c")):
+            tell(ready.at[j], axis, 1)
+            hear(ready.at[j], axis, 1)
 
     def chunk_copy(src, dst, ssem, rsem, to):
         return pltpu.make_async_remote_copy(
@@ -135,109 +264,6 @@
         return carry
 
     lax.fori_loop(1, n_sp, send_chunk, 0)
-
-    def guarded(cond, action):
-        if cond is None:
-            action()
-        else:
-            pl.when(cond)(action)
-
-    def hop(t, where, to):
-        return pltpu.make_async_remote_copy(
-            src_ref=slot(t, where), dst_ref=slot(t, where), send_sem=wsend.at[t],
-            recv_sem=wrecv.at[t, index(where)], device_id=device(to), device_id_type=MESH)
-
-    def across(t, ref):
-        return pltpu.make_async_remote_copy(
-            src_ref=ref, dst_ref=ref, send_sem=ssend.at[t], recv_sem=srecv.at[t],
-            device_id=device(dict(at, c=1 - at["c"])), device_id_type=MESH)
-
-    def source(move):
-        where, cond = dict(at), None
-        for axis, m in move.items():
-            n, i = dims[axis], at[axis]
-            if n == 2:
-                where[axis] = 1 - i if m else i
-            elif m:
-                here = jnp.logical_and(i - m >= 0, i - m < n)
-                cond = here if cond is None else jnp.logical_and(cond, here)
-                where[axis] = jnp.clip(i - m, 0, n - 1)
-        return where, cond
-
-    def onward(order, move, level):
-        found = []
-        for deeper in range(level, len(order)):
-            axis = order[deeper]
-            n, m = dims[axis], move[axis]
-            if n == 2:
-                ways = () if m else (1,)
-            else:
-                ways = (1, -1) if m == 0 else ((m // abs(m),) if abs(m) < n - 1 else ())
-            found += [(axis, way, deeper) for way in ways]
-        return found
-
-    def forward(t, move, level, first=False):
-        where, cond = source(move)
-
-        def act():
-            if not first:
-                hop(t, where, at).wait_recv()
-            for axis, way, _ in onward(ORDERS[t], move, level):
-                n, i = dims[axis], at[axis]
-                if n == 2:
-                    hop(t, where, dict(at, **{axis: 1 - i})).start()
-                else:
-                    ok = (i < n - 1) if way == 1 else (i > 0)
-                    to = dict(at, **{axis: jnp.clip(i + way, 0, n - 1)})
-                    pl.when(ok)(lambda to=to: hop(t, where, to).start())
-            across(t, slot(t, where)).start()
-
-        guarded(cond, act)
-
-    def sends(t, z):
-        total, wave = 0, [({axis: 0 for axis in ORDERS[t]}, 0)]
-        while wave:
-            later = []
-            for move, level in wave:
-                valid = 0 <= z - move["z"] < nz
-                for axis, way, deeper in onward(ORDERS[t], move, level):
-                    total += valid and (axis != "z" or 0 <= z + way < nz)
-                    later.append((dict(move, **{axis: move[axis] + way}), deeper))
-            wave = later
-        return total
-
-    def plan():
-        waves, current = [], [(t, {axis: 0 for axis in ORDERS[t]}, 0) for t in pieces]
-        depth = 0
-        while current:
-            later = []
-            for t, move, level in current:
-                for axis, way, deeper in onward(ORDERS[t], move, level):
-                    later.append((t, dict(move, **{axis: move[axis] + way}), deeper))
-            waves += [(depth + LAG * event[0], event) for event in later]
-            current, depth = later, depth + 1
-        return [event for _, event in sorted(waves, key=lambda found: found[0])]
-
-    def toss(t, d):
-        to = lax.rem(me * n_dp + mx + d, n_sp * n_dp)
-        return pltpu.make_async_remote_copy(
-            src_ref=slot(t, at), dst_ref=slot(t, at), send_sem=wsend.at[t], recv_sem=wrecv.at[t, 0],
-            device_id={"sp": to // n_dp, "dp": lax.rem(to, n_dp)}, device_id_type=MESH)
-
-    for copy in local:
-        copy.wait()
-    events = []
-    if paired:
-        events = plan()
-        for t in pieces:
-            forward(t, {axis: 0 for axis in ORDERS[t]}, 0, True)
-    else:
-        for t in pieces:
-            def toss_one(d, carry, t=t):
-                toss(t, d).start()
-                return carry
-
-            lax.fori_loop(1, n_sp * n_dp, toss_one, 0)
 
     for copy in loads[1:]:
         copy.wait()
@@ -296,8 +322,8 @@
     def dot_t(a, b):
         return lax.dot_general(a, b, (((1,), (1,)), ((), ())), preferred_element_type=F32)
 
-    inside = int(len(events) * SHARE)
-    cuts = [inside * k // n_sp for k in range(n_sp + 1)]
+    cuts = [0] + [int(len(events) * (PRE + (SHARE - PRE) * k / (n_sp - 1))) for k in range(n_sp)]
+    inside = cuts[-1]
 
     def block(k, carry):
         for i in range(n_sp):
@@ -451,7 +477,7 @@
             pltpu.VMEM((6, n_sp, states), F32),
             pltpu.VMEM((2 * fold, LANES, states), BF16),
             pltpu.VMEM((2, wd, states), F32),
-            sem((len(ORDERS),)), sem((len(operands),)),
+            pltpu.SemaphoreType.REGULAR((4,)), sem((len(ORDERS),)), sem((len(operands),)),
             sem((len(ORDERS),)), sem((len(ORDERS), marks)), sem((len(ORDERS),)), sem((len(ORDERS),)),
             sem((1,)), sem((n_sp,)), sem((1,)), sem((1,)),
         ],

time: 55.3 us -> 53.3 us (0.964)
  Pallas kernels: 54.2 us -> 52.2 us
    pallas_call x1, Pallas kernels: 54.2 us -> 52.2 us  [per_device(): pl.pallas_call(functools.partial(kernel, dims, (n_sp, n_dp, tokens, wd, f...]
where the time goes in v3:
time: 53.3 us; the launch traced here: 53.2 us
  Pallas kernels  52.2 us (98%)
  local copies, waits for them, and re-layouts  0.97 us (2%)
    pallas_call x1, Pallas kernels, per_device(): pl.pallas_call(functools.partial(kernel, dims, (n_sp, n_dp, tokens, wd, f...  52.2 us

profile of v3, /device:TPU:0, one launch (start us, length us, event | category | flops | bytes accessed | tf_op | source)
XLA Modules:
  0.0 53.2 jit_solution(9761589931280889368)
XLA Ops:
  0.0 52.2 %shard_map.127 = bf16[128,4096]{1,0:T(8,128)(2,1)S(1)} custom-call(bf16[128,1024]{1,0:T(8,128)(2,1)} %bitcast.8, f32[4,64]{1,0:T(4,128)} %a_real_hbm.1, f32[4,64]{1,0:T(4,128)} %a_imag_hbm.1, f32[1,2,4,64]{3,2,1,0:T(4,128)} %init_hbm.1, f32[4,2,16,64]{3,2,1,0:T(8,128)} %bitcast.9, f32[4,2,16,64]{3,2,1,0:T(8,128)} %out_map_hbm.1, f32[1,4]{1,0:T(1,128)} %bitcast.12, ...), custom_call_target="tpu_custom_call" | custom-call | tf_op jit(solution)/shard_map/pallas_call | solution.py:469
  52.2 1.0 %copy.15 = bf16[1,128,4096]{2,1,0:T(8,128)(2,1)} copy(bf16[1,128,4096]{2,1,0:T(8,128)(2,1)S(1)} %bitcast.7) | data formatting | bytes 2097152

commit v4 on v3

--- a/solution.py
+++ b/solution.py
@@ -14,10 +14,12 @@
 LANES = 128
 ORDERS = (("z", "y", "x"), ("z", "y", "x"), ("x", "z", "y"), ("y", "z", "x"), ("z", "x", "y"))
 CUTS = len(ORDERS) - 1
-SHARE = 0.5
-PRE = 0.14
+SHARE = 0.68
+PRE = 0.32
+EARLY = 0
+TOGETHER = 4
 LAGS = (0.0, 0.2, 0.4, 0.6, 0.8)
-AHEAD = 3
+AHEAD = 4
 VMEM_LIMIT = 56 * 1024 * 1024
 
 
@@ -244,6 +246,9 @@
     if paired:
         if dims["z"] > 2:
             for way in (1, -1):
+                if way == -1:
+                    for event in events[:EARLY]:
+                        forward(*event)
                 hear(ready.at[0 if way == 1 else 1], "z", -way)
                 tell(ready.at[0 if way == 1 else 1], "z", way)
         else:
@@ -322,23 +327,12 @@
     def dot_t(a, b):
         return lax.dot_general(a, b, (((1,), (1,)), ((), ())), preferred_element_type=F32)
 
-    cuts = [0] + [int(len(events) * (PRE + (SHARE - PRE) * k / (n_sp - 1))) for k in range(n_sp)]
+    cuts = [EARLY if paired else 0] + [int(len(events) * (PRE + (SHARE - PRE) * k / (n_sp - 1))) for k in range(n_sp)]
+    cuts = [max(cuts[0], cut) for cut in cuts]
     inside = cuts[-1]
 
-    def block(k, carry):
-        for i in range(n_sp):
-            if cuts[i] < cuts[i + 1]:
-                @pl.when(k == i)
-                def _():
-                    for event in events[cuts[i]:cuts[i + 1]]:
-                        forward(*event)
-
-        @pl.when(k != me)
-        def _():
-            chunk_copy(tx.at[me], rx.at[k], xsend.at[0], xrecv.at[k], me).wait_recv()
-
-        before_re, before_im = carry
-        br, bi, gr, gi, cr, ci = [bars[j, pl.ds(k, 1), :] for j in range(6)]
+    def injected(k):
+        gr, gi, cr, ci = [bars[j, pl.ds(k, 1), :] for j in range(2, 6)]
         chunk = rx[k]
         drive_re = (cr * inm[0] - ci * inm[1]).astype(BF16)
         drive_im = (cr * inm[1] + ci * inm[0]).astype(BF16)
@@ -351,24 +345,52 @@
 
         up_re, up_im = powers(gr, gi, tokens)
         sum_re, sum_im = cmul(inject(drive_re), inject(drive_im), up_re, up_im)
-        sum_re, sum_im = dot(tri, sum_re.astype(BF16)), dot(tri, sum_im.astype(BF16))
-        first_re, first_im = cmul(br, bi, before_re, before_im)
+        return dot(tri, sum_re.astype(BF16)), dot(tri, sum_im.astype(BF16))
+
+    def advanced(k, sums, carry):
+        br, bi = bars[0, pl.ds(k, 1), :], bars[1, pl.ds(k, 1), :]
+        first_re, first_im = cmul(br, bi, *carry)
         down_re, down_im = powers(br, bi, tokens)
-        state_re, state_im = cmul(sum_re + first_re, sum_im + first_im, down_re, down_im)
+        return cmul(sums[0] + first_re, sums[1] + first_im, down_re, down_im)
+
+    def responded(k, state_re, state_im):
         s_re, s_im = state_re.astype(BF16), state_im.astype(BF16)
-        response = skips * chunk.astype(F32)
+        response = skips * rx[k].astype(F32)
         for p in range(fold):
             lines = slice(p * rows, (p + 1) * rows)
             response = response + dot_t(s_re[lines], cmat[2 * p]) - dot_t(s_im[lines], cmat[2 * p + 1])
         atx[k] = gelu(response).astype(BF16)
 
-        @pl.when(k != me)
-        def _():
-            chunk_copy(atx.at[k], arx.at[me], asend.at[0], arecv.at[0], k).start()
-
-        return state_re[tokens - 1:], state_im[tokens - 1:]
-
-    lax.fori_loop(0, n_sp, block, (row_of(init, 0, 0), row_of(init, 0, 1)))
+    def blocks(i, carry):
+        group = [i * TOGETHER + j for j in range(TOGETHER)]
+        for lead in range(0, n_sp, TOGETHER):
+            inner = events[cuts[lead]:cuts[lead + TOGETHER]]
+            if inner:
+                @pl.when(i == lead // TOGETHER)
+                def _():
+                    for event in inner:
+                        forward(*event)
+
+        for k in group:
+            @pl.when(k != me)
+            def _():
+                chunk_copy(tx.at[me], rx.at[k], xsend.at[0], xrecv.at[k], me).wait_recv()
+
+        sums = [injected(k) for k in group]
+        states = []
+        for k, found in zip(group, sums):
+            states.append(advanced(k, found, carry))
+            carry = tuple(part[tokens - 1:] for part in states[-1])
+        for k, state in zip(group, states):
+            responded(k, *state)
+        for k in group:
+            @pl.when(k != me)
+            def _():
+                chunk_copy(atx.at[k], arx.at[me], asend.at[0], arecv.at[0], k).start()
+
+        return carry
+
+    lax.fori_loop(0, n_sp // TOGETHER, blocks, (row_of(init, 0, 0), row_of(init, 0, 1)))
 
     most = n_sp - 1
 
@@ -455,7 +477,7 @@
     states = groups * entries
     fold = LANES // wd
     rows = tokens // fold
-    assert signal.shape[0] == 1 and pace.shape[1] == n_sp and n_sp % 4 == 0
+    assert signal.shape[0] == 1 and pace.shape[1] == n_sp and n_sp % 4 == 0 and n_sp % TOGETHER == 0
     dims = {"x": n_dp, "c": 2, "y": 2, "z": n_sp // 4}
     wrows = w_out.shape[0]
     gcols, ocols = w_glu.shape[1], w_out.shape[1] // CUTS

time: 53.3 us -> 51.9 us (0.974)
  Pallas kernels: 52.2 us -> 50.8 us
    pallas_call x1, Pallas kernels: 52.2 us -> 50.8 us  [per_device(): pl.pallas_call(functools.partial(kernel, dims, (n_sp, n_dp, tokens, wd, f...]
where the time goes in v4:
time: 51.9 us; the launch traced here: 51.7 us
  Pallas kernels  50.8 us (98%)
  local copies, waits for them, and re-layouts  0.97 us (2%)
    pallas_call x1, Pallas kernels, per_device(): pl.pallas_call(functools.partial(kernel, dims, (n_sp, n_dp, tokens, wd, f...  50.8 us

profile of v4, /device:TPU:0, one launch (start us, length us, event | category | flops | bytes accessed | tf_op | source)
XLA Modules:
  0.0 51.7 jit_solution(14700001208217511743)
XLA Ops:
  0.0 50.8 %shard_map.127 = bf16[128,4096]{1,0:T(8,128)(2,1)S(1)} custom-call(bf16[128,1024]{1,0:T(8,128)(2,1)} %bitcast.8, f32[4,64]{1,0:T(4,128)} %a_real_hbm.1, f32[4,64]{1,0:T(4,128)} %a_imag_hbm.1, f32[1,2,4,64]{3,2,1,0:T(4,128)} %init_hbm.1, f32[4,2,16,64]{3,2,1,0:T(8,128)} %bitcast.9, f32[4,2,16,64]{3,2,1,0:T(8,128)} %out_map_hbm.1, f32[1,4]{1,0:T(1,128)} %bitcast.12, ...), custom_call_target="tpu_custom_call" | custom-call | tf_op jit(solution)/shard_map/pallas_call | solution.py:491
  50.8 1.0 %copy.15 = bf16[1,128,4096]{2,1,0:T(8,128)(2,1)} copy(bf16[1,128,4096]{2,1,0:T(8,128)(2,1)S(1)} %bitcast.7) | data formatting | bytes 2097152

commit v5 on v4

--- a/solution.py
+++ b/solution.py
@@ -265,7 +265,7 @@
 
     def send_chunk(d, carry):
         to = lax.rem(me + d, n_sp)
-        chunk_copy(tx.at[to], rx.at[me], xsend.at[0], xrecv.at[me], to).start()
+        chunk_copy(tx.at[to], rx.at[me], xsend.at[0], xrecv.at[me // TOGETHER], to).start()
         return carry
 
     lax.fori_loop(1, n_sp, send_chunk, 0)
@@ -371,10 +371,14 @@
                     for event in inner:
                         forward(*event)
 
-        for k in group:
-            @pl.when(k != me)
-            def _():
-                chunk_copy(tx.at[me], rx.at[k], xsend.at[0], xrecv.at[k], me).wait_recv()
+        def await_chunks(count):
+            some = rx.at[pl.ds(0, count)]
+            chunk_copy(some, some, xsend.at[0], xrecv.at[i], me).wait_recv()
+
+        mine = i == me // TOGETHER
+        pl.when(jnp.logical_not(mine))(lambda: await_chunks(TOGETHER))
+        if TOGETHER > 1:
+            pl.when(mine)(lambda: await_chunks(TOGETHER - 1))
 
         sums = [injected(k) for k in group]
         states = []
@@ -501,7 +505,7 @@
             pltpu.VMEM((2, wd, states), F32),
             pltpu.SemaphoreType.REGULAR((4,)), sem((len(ORDERS),)), sem((len(operands),)),
             sem((len(ORDERS),)), sem((len(ORDERS), marks)), sem((len(ORDERS),)), sem((len(ORDERS),)),
-            sem((1,)), sem((n_sp,)), sem((1,)), sem((1,)),
+            sem((1,)), sem((n_sp // TOGETHER,)), sem((1,)), sem((1,)),
         ],
         compiler_params=pltpu.CompilerParams(
             collective_id=0, has_side_effects=True, vmem_limit_bytes=VMEM_LIMIT),

time: 51.9 us -> 51.8 us (level)
  no operation moved by 1% of the time
where the time goes in v5:
time: 51.8 us; the launch traced here: 51.6 us
  Pallas kernels  50.7 us (98%)
  local copies, waits for them, and re-layouts  0.97 us (2%)
    pallas_call x1, Pallas kernels, per_device(): pl.pallas_call(functools.partial(kernel, dims, (n_sp, n_dp, tokens, wd, f...  50.7 us

profile of v5, /device:TPU:0, one launch (start us, length us, event | category | flops | bytes accessed | tf_op | source)
XLA Modules:
  0.0 51.6 jit_solution(12658035045289161078)
XLA Ops:
  0.0 50.7 %shard_map.127 = bf16[128,4096]{1,0:T(8,128)(2,1)S(1)} custom-call(bf16[128,1024]{1,0:T(8,128)(2,1)} %bitcast.8, f32[4,64]{1,0:T(4,128)} %a_real_hbm.1, f32[4,64]{1,0:T(4,128)} %a_imag_hbm.1, f32[1,2,4,64]{3,2,1,0:T(4,128)} %init_hbm.1, f32[4,2,16,64]{3,2,1,0:T(8,128)} %bitcast.9, f32[4,2,16,64]{3,2,1,0:T(8,128)} %out_map_hbm.1, f32[1,4]{1,0:T(1,128)} %bitcast.12, ...), custom_call_target="tpu_custom_call" | custom-call | tf_op jit(solution)/shard_map/pallas_call | solution.py:495
  50.7 1.0 %copy.15 = bf16[1,128,4096]{2,1,0:T(8,128)(2,1)} copy(bf16[1,128,4096]{2,1,0:T(8,128)(2,1)S(1)} %bitcast.7) | data formatting | bytes 2097152
